TPU v7x, 512 devices: a whole 4x4x16 slice. The times are simulated.
512 devices in a mesh: rep: 2 (over z_hi), fs: 32 (over z_lo, y), tp: 8 (over x, core).
Axes of the slice: x: 4, y: 4, z: 16 (z_hi: 2, z_lo: 8; z = z_hi * 8 + z_lo), core: 2. Of those that a mesh axis runs over, the one named last changes fastest.
Arguments:
- input_activation_entries: bfloat16 [24576, 2048], P(('rep', 'fs')), may hold values from -6 to 6
- premixing_rescale_factor: float32 [2048], replicated, may hold values from 0.1 to 1.9
- probe_weight_table: float32 [2048, 1024], P('fs', 'tp'), may hold values from -0.125 to 0.125
- probe_factor_list: float32 [1024], P('tp'), may hold values from 0.5 to 2
- lookup_weight_table: float32 [2048, 1024], P('fs', 'tp'), may hold values from -0.125 to 0.125
- lookup_factor_list: float32 [1024], P('tp'), may hold values from 0.5 to 2
- forget_weight_table: float32 [2048, 1024], P('fs', 'tp'), may hold values from -0.125 to 0.125
- forget_factor_list: float32 [1024], P('tp'), may hold values from 1 to 8
- forget_shift_term: float32 [1024], P('tp'), may hold values from -3 to 7
- extra_forget_logs: float32 [24576, 8], P(('rep', 'fs'), 'tp'), may hold values from -0.7 to 0
- content_weight_table: float32 [2048, 2048], P('fs', 'tp'), may hold values from -0.125 to 0.125
- content_factor_list: float32 [2048], P('tp'), may hold values from 0.5 to 2
- filter_weight_table: float32 [2048, 2048], P('fs', 'tp'), may hold values from -0.125 to 0.125
- filter_factor_list: float32 [2048], P('tp'), may hold values from 0.5 to 2
- per_group_rescale_factor: float32 [2048], P('tp'), may hold values from 0.1 to 1.9
- emission_weight_table: float32 [2048, 2048], P('tp', 'fs'), may hold values from -0.125 to 0.125
- emission_factor_list: float32 [2048], P('fs'), may hold values from 0.5 to 2
- perceptron_prenorm_factor: float32 [2048], replicated, may hold values from 0.1 to 1.9
- raising_weight_table: float32 [2048, 8192], P('fs', 'tp'), may hold values from -0.125 to 0.125
- raising_factor_list: float32 [8192], P('tp'), may hold values from 0.5 to 2
- lowering_weight_table: float32 [8192, 2048], P('tp', 'fs'), may hold values from -0.0625 to 0.0625
- lowering_factor_list: float32 [2048], P('fs'), may hold values from 0.5 to 2
Outputs:
- layer_out: bfloat16 [24576, 2048], P(('rep', 'fs'))
All inputs are finite; a program needn't handle non-finite values.
Results may differ from a plain program's by a relative error of at most 0.02.
Values may be sent and summed in bfloat16 or wider, within the bound.
No kernel may reach another device: no remote copies, remote signals or barrier semaphores. Data moves between devices by JAX's collectives and lax.ppermute only.
A program may use at most 64 MiB of HBM per device.

v0:
```python
import jax
import jax.numpy as jnp
from jax import lax
from jax.sharding import PartitionSpec as P

LOOKUP_FEATURES = 128
BLOCK = 64
epsilon = 1e-06
filter_rescaled_entries = 16.0
highest = lax.Precision.HIGHEST


def rows_first(arrays, axis, dims):
    turned = [jnp.moveaxis(a, dim, 0) for a, dim in zip(arrays, dims)]
    widths = [t[0].size for t in turned]
    both = jnp.concatenate([t.reshape(-1, w) for t, w in zip(turned, widths)], axis=1)
    filled = lax.all_gather(both, axis, axis=0, tiled=True)
    pieces = jnp.split(filled, [sum(widths[:k]) for k in range(1, len(widths))], axis=1)
    return tuple(
        (
            jnp.moveaxis(b.reshape(-1, *t.shape[1:]), 0, dim)
            for b, t, dim in zip(pieces, turned, dims)
        )
    )


def cut_along(value, dim, devices):
    before, after = (value.shape[:dim], value.shape[dim + 1 :])
    return jnp.moveaxis(value.reshape(*before, devices, -1, *after), dim, 0)


def sent_and_summed(value, axis, dim):
    pieces = cut_along(value, dim, lax.axis_size(axis))
    arrived = lax.all_to_all(pieces, axis, split_axis=0, concat_axis=0, tiled=True)
    return arrived.astype(jnp.float32).sum(axis=0)


def laid_out(pieces, dim):
    dims = list(pieces.shape[1:])
    dims[dim] *= pieces.shape[0]
    return jnp.moveaxis(pieces, 0, dim).reshape(dims)


def from_everyone(value, axis):
    devices = lax.axis_size(axis)
    return lax.all_to_all(
        jnp.broadcast_to(value[None], (devices, *value.shape)), axis, 0, 0, tiled=True
    )


def gathered_copies(value, axis, dim):
    return laid_out(from_everyone(value, axis), dim)


def rms_rows(matrix, gain):
    matrix = matrix.astype(jnp.float32)
    return matrix * lax.rsqrt(jnp.mean(matrix * matrix, axis=-1, keepdims=True) + epsilon) * gain


def recur_head(queries, keys_in, vals, forget_log_rate):
    length = queries.shape[0]
    blocks = length // BLOCK

    def to_blocks(tensor):
        return tensor.astype(jnp.float32).reshape(blocks, BLOCK, tensor.shape[-1])

    causal = jnp.tril(jnp.ones((BLOCK, BLOCK), dtype=bool))[:, :, None]

    def advance(memory, inputs):
        query_block, key_block, value_block, decay_block = inputs
        cumulative = jnp.cumsum(decay_block, axis=0)
        spread = cumulative[:, None, :] - cumulative[None, :, :]
        weights = jnp.exp(jnp.where(causal, spread, -jnp.inf))
        scores = jnp.einsum("tc,sc,tsc->ts", query_block, key_block, weights, precision=highest)
        within = jnp.dot(scores, value_block, precision=highest)
        carried = jnp.dot(query_block * jnp.exp(cumulative), memory, precision=highest)
        closing = cumulative[-1]
        scaled_keys = key_block * jnp.exp(closing[None, :] - cumulative)
        memory = jnp.exp(closing)[:, None] * memory + jnp.dot(
            scaled_keys.T, value_block, precision=highest
        )
        return (memory, within + carried)

    initial = jnp.zeros((queries.shape[-1], vals.shape[-1]), jnp.float32)
    _, outputs = lax.scan(
        advance,
        initial,
        (to_blocks(queries), to_blocks(keys_in), to_blocks(vals), to_blocks(forget_log_rate)),
    )
    return outputs.reshape(length, vals.shape[-1])


def per_group_mixing_values(
    probe_mapped_entries,
    lookup_mapped_entries,
    forget_mapped_entries,
    content_mapped_entries,
    filter_mapped_entries,
    forget_shift_term,
    extra_forget_logs,
    per_group_rescale_factor,
):
    group_count_total = extra_forget_logs.shape[-1]
    queries = (jax.nn.silu(probe_mapped_entries) * LOOKUP_FEATURES ** (-0.5)).astype(jnp.bfloat16)
    keyed = jax.nn.silu(lookup_mapped_entries).astype(jnp.bfloat16)
    valued = jax.nn.silu(content_mapped_entries).astype(jnp.bfloat16)
    forget_log_rate = jax.nn.log_sigmoid(
        forget_mapped_entries + forget_shift_term
    ) / filter_rescaled_entries + jnp.repeat(extra_forget_logs, LOOKUP_FEATURES, axis=1)

    def by_head(tensor):
        return tensor.reshape(tensor.shape[0], group_count_total, -1).transpose(1, 0, 2)

    outputs = jax.vmap(recur_head)(
        by_head(queries), by_head(keyed), by_head(valued), by_head(forget_log_rate)
    )
    outputs = outputs * lax.rsqrt(jnp.mean(outputs * outputs, axis=-1, keepdims=True) + epsilon)
    merged = outputs.transpose(1, 0, 2).reshape(outputs.shape[1], -1)
    return (merged * per_group_rescale_factor * jax.nn.silu(filter_mapped_entries)).astype(
        jnp.bfloat16
    )


def body(
    input_activation_entries,
    premixing_rescale_factor,
    probe_weight_table,
    probe_factor_list,
    lookup_weight_table,
    lookup_factor_list,
    forget_weight_table,
    forget_factor_list,
    forget_shift_term,
    extra_forget_logs,
    content_weight_table,
    content_factor_list,
    filter_weight_table,
    filter_factor_list,
    per_group_rescale_factor,
    emission_weight_table,
    emission_factor_list,
    perceptron_prenorm_factor,
    raising_weight_table,
    raising_factor_list,
    lowering_weight_table,
    lowering_factor_list,
):
    whole_out_scale, whole_down_scale = rows_first(
        (emission_factor_list, lowering_factor_list), "fs", (0, 0)
    )
    normed = rms_rows(input_activation_entries, premixing_rescale_factor).astype(jnp.bfloat16)
    query_bf = probe_weight_table.astype(jnp.bfloat16)
    key_bf = lookup_weight_table.astype(jnp.bfloat16)
    decay_bf = forget_weight_table.astype(jnp.bfloat16)
    value_bf = content_weight_table.astype(jnp.bfloat16)
    gate_bf = filter_weight_table.astype(jnp.bfloat16)
    out_bf = emission_weight_table.astype(jnp.bfloat16)
    up_bf = raising_weight_table.astype(jnp.bfloat16)
    down_bf = lowering_weight_table.astype(jnp.bfloat16)
    share_rows = input_activation_entries.shape[0] // lax.axis_size("tp")
    share_start = lax.axis_index("tp") * share_rows
    collected = rows_first(
        (query_bf, key_bf, decay_bf, value_bf, gate_bf, up_bf, out_bf, down_bf),
        "fs",
        (0, 0, 0, 0, 0, 0, 1, 1),
    )
    projected = tuple(
        (jnp.dot(normed, matrix, preferred_element_type=jnp.float32) for matrix in collected[:5])
    )
    mixing_product = per_group_mixing_values(
        projected[0] * probe_factor_list,
        projected[1] * lookup_factor_list,
        projected[2] * forget_factor_list,
        projected[3] * content_factor_list,
        projected[4] * filter_factor_list,
        forget_shift_term,
        extra_forget_logs,
        per_group_rescale_factor,
    )
    mix_part = (
        jnp.dot(mixing_product, collected[6], preferred_element_type=jnp.float32) * whole_out_scale
    )
    mix_rounded = lax.optimization_barrier(mix_part.astype(jnp.bfloat16)).astype(jnp.float32)
    mix_share = sent_and_summed(mix_rounded.astype(jnp.bfloat16), "tp", 0)
    token_share = lax.dynamic_slice_in_dim(input_activation_entries, share_start, share_rows, 0)
    residual = (token_share.astype(jnp.float32) + mix_share).astype(jnp.bfloat16)
    normed_share = rms_rows(residual, perceptron_prenorm_factor).astype(jnp.bfloat16)
    normed_mlp = gathered_copies(normed_share, "tp", 0)
    lifted = jnp.dot(normed_mlp, collected[5], preferred_element_type=jnp.float32)
    hidden = jnp.square(jax.nn.relu(lifted * raising_factor_list)).astype(jnp.bfloat16)
    mlp_part = jnp.dot(hidden, collected[7], preferred_element_type=jnp.float32) * whole_down_scale
    mlp_rounded = lax.optimization_barrier(mlp_part.astype(jnp.bfloat16)).astype(jnp.float32)
    mlp_share = sent_and_summed(mlp_rounded.astype(jnp.bfloat16), "tp", 0)
    out_share = (residual.astype(jnp.float32) + mlp_share).astype(jnp.bfloat16)
    return gathered_copies(out_share, "tp", 0)


def solution(mesh):
    return jax.shard_map(
        body,
        mesh=mesh,
        in_specs=(
            P(("rep", "fs"), None),
            P(),
            P("fs", "tp"),
            P("tp"),
            P("fs", "tp"),
            P("tp"),
            P("fs", "tp"),
            P("tp"),
            P("tp"),
            P(("rep", "fs"), "tp"),
            P("fs", "tp"),
            P("tp"),
            P("fs", "tp"),
            P("tp"),
            P("tp"),
            P("tp", "fs"),
            P("fs"),
            P(),
            P("fs", "tp"),
            P("tp"),
            P("tp", "fs"),
            P("fs"),
        ),
        out_specs=P(("rep", "fs"), None),
        check_vma=False,
    )
```

profile of v0, /device:TPU:1, one launch (start us, length us, event | category | flops | bytes accessed | tf_op | source)
XLA Modules:
  0.0 413.1 jit_solution(14367460227402730513)
XLA Ops:
  6.5 0.9 constant_dynamic-update-slice_fusion.2
  7.4 0.8 constant_dynamic-update-slice_fusion.1
  8.2 0.8 constant_dynamic-update-slice_fusion
  9.0 0.8 convert_dynamic-update-slice_fusion.2
  9.8 0.8 convert_dynamic-update-slice_fusion.1
  10.6 1.0 convert_dynamic-update-slice_fusion
  11.6 0.8 bitcast_dynamic-update-slice_fusion.1
  12.5 1.0 bitcast_dynamic-update-slice_fusion
  13.4 0.8 copy-done.3
  14.3 0.7 maximum_bitcast_fusion
  15.0 114.9 %all-gather = f32[32,64,2]{1,2,0:T(2,128)S(1)} all-gather(f32[1,64,2]{1,2,0:T(2,128)S(1)} %maximum_bitcast_fusion), channel_id=1, replica_groups=mesh['rep'=2,'fs'=32,'tp'=8] {'fs'}, dimensions={0}, use_global_device_ids=true | all-gather | bytes 16896 | tf_op jit(solution)/shard_map/all_gather | solution.py:17
  129.9 0.7 reduce.3
  130.6 0.4 fusion.35
  131.1 0.4 fusion.37
  131.5 115.5 %all-gather.3.cloned.1.call-done = bf16[2048,3200]{1,0:T(8,128)(2,1)} async-done(((bf16[64,3200]{1,0:T(8,128)(2,1)}), bf16[2048,3200]{1,0:T(8,128)(2,1)}) %all-gather.3.cloned.1.call-update) | async-done | bytes 13107216 | tf_op jit(solution)/shard_map/all_gather | solution.py:17
  247.0 1.8 multiply_convert_fusion.3
  248.9 2.2 multiply_convert_fusion.5
  251.2 1.6 multiply_convert_fusion.4
  252.9 1.7 fusion.67
  254.7 20.3 %while.13 = (s32[]{:T(128)}, f32[1,128,256]{2,1,0:T(8,128)S(1)}, f32[6,1,64,256]{3,2,1,0:T(8,128)S(1)}, f32[6,1,64,128]{3,2,1,0:T(8,128)S(1)}, f32[6,1,64,128]{3...) while((s32[]{:T(128)}, f32[1,128,256]{2,1,0:T(8,128)S(1)}, ...), condition=%wide.region_3.4_spmd.clone, body=%wide.region_1.3_spmd.clone.sunk | while | flops 66224128 | bytes 5469312 | solution.py:85
  254.8 0.6 select_exponential_fusion.2
  255.5 1.7 fusion.105
  257.2 0.3 fusion.106
  257.4 0.2 fusion.107
  257.7 0.4 fusion.103
  258.2 0.6 select_exponential_fusion.2
  258.8 1.7 fusion.105
  260.5 0.3 fusion.106
  260.8 0.2 fusion.107
  261.1 0.4 fusion.103
  261.6 0.6 select_exponential_fusion.2
  262.2 1.7 fusion.105
  263.9 0.3 fusion.106
  264.2 0.2 fusion.107
  264.4 0.4 fusion.103
  265.0 0.6 select_exponential_fusion.2
  265.6 1.7 fusion.105
  267.3 0.3 fusion.106
  267.6 0.2 fusion.107
  267.8 0.4 fusion.103
  268.4 0.6 select_exponential_fusion.2
  269.0 1.7 fusion.105
  270.7 0.3 fusion.106
  271.0 0.2 fusion.107
  271.2 0.4 fusion.103
  271.7 0.6 select_exponential_fusion.2
  272.4 1.7 fusion.105
  274.1 0.3 fusion.106
  274.4 0.2 fusion.107
  274.6 0.4 fusion.103
  275.2 2.3 fusion.60
  277.5 3.0 multiply_convert_fusion.1
  280.5 23.9 %all-to-all-start = ((bf16[8,48,2048]{2,1,0:T(8,128)(2,1)}), bf16[8,48,2048]{2,1,0:T(8,128)(2,1)S(1)}, u32[]{:S(2)}, u32[]{:S(2)}) async-start(bf16[8,48,2048]{2,1,0:T(8,128)(2,1)} %bitcast.150), calls=%async_computation | async-start | bytes 3145728 | tf_op jit(solution)/shard_map/all_to_all | solution.py:34
  304.4 20.6 %all-to-all-done = bf16[8,48,2048]{2,1,0:T(8,128)(2,1)S(1)} async-done(((bf16[8,48,2048]{2,1,0:T(8,128)(2,1)}), bf16[8,48,2048]{2,1,0:T(8,128)(2,1)S(1)}, u32[]{:S(2)}, u32[]{:S(2)}) %all-to-all-start) | async-done | bytes 1572896 | tf_op jit(solution)/shard_map/all_to_all | solution.py:34
  325.0 0.2 convert_reduce_fusion.1
  325.3 0.2 fusion.54
  325.6 0.2 broadcast_in_dim.33
  325.8 24.0 %all_to_all.20 = bf16[8,48,2048]{2,1,0:T(8,128)(2,1)S(1)} all-to-all(bf16[8,48,2048]{2,1,0:T(8,128)(2,1)S(1)} %broadcast_in_dim.33), channel_id=1, replica_groups=mesh['rep'=2,'fs'=32,'tp'=8] {'tp'}, dimensions={0} | all-to-all | bytes 3145728 | tf_op jit(solution)/shard_map/all_to_all | solution.py:46
  349.7 6.9 %multiply_convert_fusion = bf16[384,2048]{1,0:T(8,128)(2,1)S(1)} fusion(bf16[2048,3200]{1,0:T(8,128)(2,1)} %all-gather.3.cloned.1.call-done, f32[2048]{0:T(1024)S(1)} %bitcast.157, bf16[384,2048]{1,0:T(8,128)(2,1)S(1)} %bitcast.151, f32[1024]{0:T(1024)S(1)} %copy-done.7), kind=kOutput, calls=%fused_computation.49 | convolution fusion | flops 3224371200 | bytes 11546624 | tf_op jit(solution)/shard_map/dot_general | solution.py:191
  356.6 24.0 %all_to_all.21 = bf16[8,48,2048]{2,1,0:T(8,128)(2,1)S(1)} all-to-all(bf16[8,48,2048]{2,1,0:T(8,128)(2,1)S(1)} %bitcast.152), channel_id=1, replica_groups=mesh['rep'=2,'fs'=32,'tp'=8] {'tp'}, dimensions={0} | all-to-all | bytes 3145728 | tf_op jit(solution)/shard_map/all_to_all | solution.py:34
  380.7 0.2 convert_reduce_fusion
  380.9 0.2 broadcast_in_dim.34
  381.1 24.0 %all_to_all.22 = bf16[8,48,2048]{2,1,0:T(8,128)(2,1)S(1)} all-to-all(bf16[8,48,2048]{2,1,0:T(8,128)(2,1)S(1)} %broadcast_in_dim.34), channel_id=1, replica_groups=mesh['rep'=2,'fs'=32,'tp'=8] {'tp'}, dimensions={0} | all-to-all | bytes 3145728 | tf_op jit(solution)/shard_map/all_to_all | solution.py:46
  405.1 1.1 copy.74
  (82 shorter events, 1.5 us)
Async XLA Ops:
  6.5 124.1 %copy-start = (bf16[384,2048]{1,0:T(8,128)(2,1)S(1)}, bf16[384,2048]{1,0:T(8,128)(2,1)}, u32[]{:S(2)}) copy-start(bf16[384,2048]{1,0:T(8,128)(2,1)} %param.24) | copy-start | bytes 4718596
  6.5 124.5 %copy-start.5 = (f32[2048]{0:T(1024)S(1)}, f32[2048]{0:T(1024)}, u32[]{:S(2)}) copy-start(f32[2048]{0:T(1024)} %param.25) | copy-start | bytes 24580
  6.5 240.5 %all-gather.3.cloned.1.call-start = ((), (), s32[]{:S(2)}) async-start(), calls=%async_computation.4 | async-start | bytes 13516800 | tf_op jit(solution)/shard_map/all_gather | solution.py:17
  13.4 0.8 copy-start.3
  130.6 116.4 %copy-start.8 = (f32[256]{0:T(256)S(1)}, f32[256]{0:T(256)}, u32[]{:S(2)}) copy-start(f32[256]{0:T(256)} %param.35) | copy-start | bytes 3076
  131.5 117.4 %copy-start.1 = (bf16[384,2048]{1,0:T(8,128)(2,1)}, bf16[384,2048]{1,0:T(8,128)(2,1)S(1)}, u32[]{:S(2)}) copy-start(bf16[384,2048]{1,0:T(8,128)(2,1)S(1)} %fusion.37) | copy-start | bytes 4718596
  131.5 117.4 %copy-start.11 = (f32[128]{0:T(128)S(1)}, f32[128]{0:T(128)}, u32[]{:S(2)}) copy-start(f32[128]{0:T(128)} %param.29) | copy-start | bytes 1540
  248.9 2.3 copy-start.12
  248.9 2.3 copy-start.2
  251.2 1.7 copy-start.13
  251.2 1.7 copy-start.14
  252.9 1.8 copy-start.4
  254.7 20.6 %copy-start.9 = (f32[256]{0:T(256)S(1)}, f32[256]{0:T(256)}, u32[]{:S(2)}) copy-start(f32[256]{0:T(256)} %param.37) | copy-start | bytes 3076
  254.7 20.6 %copy-start.10 = (f32[256]{0:T(256)S(1)}, f32[256]{0:T(256)}, u32[]{:S(2)}) copy-start(f32[256]{0:T(256)} %param.38) | copy-start | bytes 3076
  280.5 44.5 %all-to-all-start = ((bf16[8,48,2048]{2,1,0:T(8,128)(2,1)}), bf16[8,48,2048]{2,1,0:T(8,128)(2,1)S(1)}, u32[]{:S(2)}, u32[]{:S(2)}) async-start(bf16[8,48,2048]{2,1,0:T(8,128)(2,1)} %bitcast.150), calls=%async_computation | async-start | bytes 3145728 | tf_op jit(solution)/shard_map/all_to_all | solution.py:34
  304.4 21.0 %copy-start.6 = (f32[2048]{0:T(1024)S(1)}, f32[2048]{0:T(1024)}, u32[]{:S(2)}) copy-start(f32[2048]{0:T(1024)} %param.41) | copy-start | bytes 24580
  325.6 24.2 %copy-start.7 = (f32[1024]{0:T(1024)S(1)}, f32[1024]{0:T(1024)}, u32[]{:S(2)}) copy-start(f32[1024]{0:T(1024)} %param.43) | copy-start | bytes 12292
Sparse Core Ops, SparseCore 0:
  14.4 232.6 all-gather.2
where the time goes:
time: 414 us; the launch traced here: 413 us
  blocking collectives  187 us (45%)
  waiting for transfers between devices  136 us (33%)
  other arithmetic  24.6 us (6%)
  matrix products  24.6 us (6%)
  starting transfers between devices  23.9 us (6%)
  between operations  13.7 us (3%)
    all_gather x1, waiting for transfers between devices, rows_first(): filled = lax.all_gather(both, axis, axis=0, tiled=True)  116 us
    all_gather x1, blocking collectives, rows_first(): filled = lax.all_gather(both, axis, axis=0, tiled=True)  115 us
    all_to_all x2, blocking collectives, from_everyone(): lax.all_to_all(jnp.broadcast_to(value[None], (devices, *value.shape)), ax...  48 us
    all_to_all x1, blocking collectives, sent_and_summed(): lax.all_to_all(pieces, axis, split_axis=0, concat_axis=0, tiled=True)  24 us
    all_to_all x1, starting transfers between devices, sent_and_summed(): lax.all_to_all(pieces, axis, split_axis=0, concat_axis=0, tiled=True)  23.9 us
    all_to_all x1, waiting for transfers between devices, sent_and_summed(): lax.all_to_all(pieces, axis, split_axis=0, concat_axis=0, tiled=True)  20.6 us
    dot_general x6, other arithmetic, advance(): jnp.einsum('tc,sc,tsc->ts', query_block, key_block, weights, precision=hi...  10.2 us
    dot_general x5, matrix products, body(): jnp.dot(normed, matrix, preferred_element_type=jnp.float32)  9.67 us
  transfers between devices with their start and end apart: 2, of which 2 were waited for; matrix products, arithmetic and copies ran while one was open for 1% of the time, Pallas kernels for 0%

commit v1 on v0

--- a/solution.py
+++ b/solution.py
@@ -14,7 +14,9 @@
     turned = [jnp.moveaxis(a, dim, 0) for a, dim in zip(arrays, dims)]
     widths = [t[0].size for t in turned]
     both = jnp.concatenate([t.reshape(-1, w) for t, w in zip(turned, widths)], axis=1)
-    filled = lax.all_gather(both, axis, axis=0, tiled=True)
+    filled = jnp.concatenate(
+        lax.all_to_all(jnp.stack([both] * lax.axis_size(axis)), axis, 0, 0), axis=0
+    )
     pieces = jnp.split(filled, [sum(widths[:k]) for k in range(1, len(widths))], axis=1)
     return tuple(
         (

time: 414 us -> 764 us (1.85)
  waiting for transfers between devices: 136 us -> 601 us
  blocking collectives: 187 us -> 72 us
  between operations: 13.7 us -> 0.38 us
    all_to_all x0 -> x2, waiting for transfers between devices: none -> 581 us  [rows_first(): lax.all_to_all(jnp.stack([both] * lax.axis_size(axis)), axis, 0, 0)]
    all_gather x1 -> x0, waiting for transfers between devices: 116 us -> none  [rows_first(): filled = lax.all_gather(both, axis, axis=0, tiled=True)]
    all_gather x1 -> x0, blocking collectives: 115 us -> none  [rows_first(): filled = lax.all_gather(both, axis, axis=0, tiled=True)]
    all_to_all x0 -> x2, starting transfers between devices: none -> 23.7 us  [rows_first(): lax.all_to_all(jnp.stack([both] * lax.axis_size(axis)), axis, 0, 0)]
    all_to_all x1, starting transfers between devices: 23.9 us -> 6.67 us  [sent_and_summed(): lax.all_to_all(pieces, axis, split_axis=0, concat_axis=0, tiled=True)]
  transfers between devices with their start and end apart: 2 -> 3, of which waited for: 2 -> 3; matrix products, arithmetic and copies ran while one was open for 1% -> 1% of each run, Pallas kernels for 0% -> 0%
where the time goes in v1:
time: 764 us; the launch traced here: 763 us
  waiting for transfers between devices  601 us (79%)
  blocking collectives  72 us (9%)
  starting transfers between devices  30.4 us (4%)
  matrix products  24.6 us (3%)
  other arithmetic  24.4 us (3%)
  local copies, waits for them, and re-layouts  9.74 us (1%)
    all_to_all x2, waiting for transfers between devices, rows_first(): lax.all_to_all(jnp.stack([both] * lax.axis_size(axis)), axis, 0, 0)  581 us
    all_to_all x2, blocking collectives, from_everyone(): lax.all_to_all(jnp.broadcast_to(value[None], (devices, *value.shape)), ax...  48 us
    all_to_all x1, blocking collectives, sent_and_summed(): lax.all_to_all(pieces, axis, split_axis=0, concat_axis=0, tiled=True)  24 us
    all_to_all x2, starting transfers between devices, rows_first(): lax.all_to_all(jnp.stack([both] * lax.axis_size(axis)), axis, 0, 0)  23.7 us
    all_to_all x1, waiting for transfers between devices, sent_and_summed(): lax.all_to_all(pieces, axis, split_axis=0, concat_axis=0, tiled=True)  20.6 us
  transfers between devices with their start and end apart: 3, of which 3 were waited for; matrix products, arithmetic and copies ran while one was open for 1% of the time, Pallas kernels for 0%

profile of v1, /device:TPU:1, one launch (start us, length us, event | category | flops | bytes accessed | tf_op | source)
XLA Modules:
  0.0 763.3 jit_solution(6993578968765375652)
XLA Ops:
  0.0 0.7 pad_maximum_fusion
  0.7 0.7 reshape.293
  1.4 16.1 %all-to-all-start.1 = ((f32[32,1,128]{2,1,0:T(1,128)}), f32[32,1,128]{2,1,0:T(1,128)S(1)}, u32[]{:S(2)}, u32[]{:S(2)}) async-start(f32[32,1,128]{2,1,0:T(1,128)} %reshape.293), calls=%async_computation.1 | async-start | bytes 32768 | tf_op jit(solution)/shard_map/all_to_all | solution.py:18
  17.5 0.8 constant_dynamic-update-slice_fusion.2
  18.3 0.8 constant_dynamic-update-slice_fusion.1
  19.0 0.8 constant_dynamic-update-slice_fusion
  19.8 0.8 convert_dynamic-update-slice_fusion.2
  20.6 0.8 convert_dynamic-update-slice_fusion.1
  21.5 1.0 convert_dynamic-update-slice_fusion
  22.4 0.8 bitcast_dynamic-update-slice_fusion.1
  23.3 1.0 bitcast_dynamic-update-slice_fusion
  24.3 4.6 all-to-all-done.1
  28.9 6.4 stack.4
  35.3 7.6 %all-to-all-start = ((bf16[32,64,3200]{2,1,0:T(8,128)(2,1)}), bf16[32,64,3200]{2,1,0:T(8,128)(2,1)}, u32[]{:S(2)}, u32[]{:S(2)}) async-start(bf16[32,64,3200]{2,1,0:T(8,128)(2,1)} %stack.4), calls=%async_computation | async-start | bytes 26214400 | tf_op jit(solution)/shard_map/all_to_all | solution.py:18
  43.0 0.4 fusion.35
  43.4 0.4 fusion.37
  43.9 0.6 broadcast.125
  44.4 0.6 reduce.5
  45.2 576.1 %all-to-all-done = bf16[32,64,3200]{2,1,0:T(8,128)(2,1)} async-done(((bf16[32,64,3200]{2,1,0:T(8,128)(2,1)}), bf16[32,64,3200]{2,1,0:T(8,128)(2,1)}, u32[]{:S(2)}, u32[]{:S(2)}) %all-to-all-start) | async-done | bytes 13107232 | tf_op jit(solution)/shard_map/all_to_all | solution.py:18
  621.3 1.8 multiply_convert_fusion.3
  623.3 2.2 multiply_convert_fusion.5
  625.5 1.6 multiply_convert_fusion.4
  627.2 1.7 fusion.67
  629.0 20.3 %while.13 = (s32[]{:T(128)}, f32[1,128,256]{2,1,0:T(8,128)S(1)}, f32[6,1,64,256]{3,2,1,0:T(8,128)S(1)}, f32[6,1,64,128]{3,2,1,0:T(8,128)S(1)}, f32[6,1,64,128]{3...) while((s32[]{:T(128)}, f32[1,128,256]{2,1,0:T(8,128)S(1)}, ...), condition=%wide.region_3.4_spmd.clone, body=%wide.region_1.3_spmd.clone.sunk | while | flops 66224128 | bytes 5469312 | solution.py:87
  629.1 0.6 select_exponential_fusion.2
  629.8 1.7 fusion.105
  631.5 0.3 fusion.106
  631.7 0.2 fusion.107
  632.0 0.4 fusion.103
  632.5 0.6 select_exponential_fusion.2
  633.2 1.7 fusion.105
  634.9 0.3 fusion.106
  635.1 0.2 fusion.107
  635.4 0.4 fusion.103
  635.9 0.6 select_exponential_fusion.2
  636.5 1.7 fusion.105
  638.2 0.3 fusion.106
  638.5 0.2 fusion.107
  638.8 0.4 fusion.103
  639.3 0.6 select_exponential_fusion.2
  639.9 1.7 fusion.105
  641.6 0.3 fusion.106
  641.9 0.2 fusion.107
  642.1 0.4 fusion.103
  642.7 0.6 select_exponential_fusion.2
  643.3 1.7 fusion.105
  645.0 0.3 fusion.106
  645.3 0.2 fusion.107
  645.5 0.4 fusion.103
  646.1 0.6 select_exponential_fusion.2
  646.7 1.7 fusion.105
  648.4 0.3 fusion.106
  648.9 0.4 fusion.103
  649.5 2.3 fusion.60
  651.8 3.0 multiply_convert_fusion.1
  654.8 6.7 all-to-all-start.2
  661.5 20.6 %all-to-all-done.2 = bf16[8,48,2048]{2,1,0:T(8,128)(2,1)S(1)} async-done(((bf16[8,48,2048]{2,1,0:T(8,128)(2,1)}), bf16[8,48,2048]{2,1,0:T(8,128)(2,1)S(1)}, u32[]{:S(2)}, u32[]{:S(2)}) %all-to-all-start.2) | async-done | bytes 1572896 | tf_op jit(solution)/shard_map/all_to_all | solution.py:36
  682.1 0.2 convert_reduce_fusion.1
  682.8 24.0 %all_to_all.30 = bf16[8,48,2048]{2,1,0:T(8,128)(2,1)S(1)} all-to-all(bf16[8,48,2048]{2,1,0:T(8,128)(2,1)S(1)} %broadcast_in_dim.33), channel_id=1, replica_groups=mesh['rep'=2,'fs'=32,'tp'=8] {'tp'}, dimensions={0} | all-to-all | bytes 3145728 | tf_op jit(solution)/shard_map/all_to_all | solution.py:48
  706.8 6.9 multiply_convert_fusion
  713.7 24.0 %all_to_all.31 = bf16[8,48,2048]{2,1,0:T(8,128)(2,1)S(1)} all-to-all(bf16[8,48,2048]{2,1,0:T(8,128)(2,1)S(1)} %bitcast.154), channel_id=1, replica_groups=mesh['rep'=2,'fs'=32,'tp'=8] {'tp'}, dimensions={0} | all-to-all | bytes 3145728 | tf_op jit(solution)/shard_map/all_to_all | solution.py:36
  737.7 0.2 convert_reduce_fusion
  738.2 24.0 %all_to_all.32 = bf16[8,48,2048]{2,1,0:T(8,128)(2,1)S(1)} all-to-all(bf16[8,48,2048]{2,1,0:T(8,128)(2,1)S(1)} %broadcast_in_dim.34), channel_id=1, replica_groups=mesh['rep'=2,'fs'=32,'tp'=8] {'tp'}, dimensions={0} | all-to-all | bytes 3145728 | tf_op jit(solution)/shard_map/all_to_all | solution.py:48
  762.2 1.1 copy.80
  (88 shorter events, 2.3 us)
Async XLA Ops:
  1.4 27.5 %all-to-all-start.1 = ((f32[32,1,128]{2,1,0:T(1,128)}), f32[32,1,128]{2,1,0:T(1,128)S(1)}, u32[]{:S(2)}, u32[]{:S(2)}) async-start(f32[32,1,128]{2,1,0:T(1,128)} %reshape.293), calls=%async_computation.1 | async-start | bytes 32768 | tf_op jit(solution)/shard_map/all_to_all | solution.py:18
  35.3 7.7 %copy-start.6 = (f32[384,1]{0,1:T(1,128)S(1)}, f32[384,1]{0,1:T(1,128)}, u32[]{:S(2)}) copy-start(f32[384,1]{0,1:T(1,128)} %param.33) | copy-start | bytes 4612
  35.3 7.7 %copy-start = (bf16[384,2048]{1,0:T(8,128)(2,1)S(1)}, bf16[384,2048]{1,0:T(8,128)(2,1)}, u32[]{:S(2)}) copy-start(bf16[384,2048]{1,0:T(8,128)(2,1)} %param.24) | copy-start | bytes 4718596
  35.3 8.1 %copy-start.4 = (f32[2048]{0:T(1024)S(1)}, f32[2048]{0:T(1024)}, u32[]{:S(2)}) copy-start(f32[2048]{0:T(1024)} %param.25) | copy-start | bytes 24580
  35.3 586.0 %all-to-all-start = ((bf16[32,64,3200]{2,1,0:T(8,128)(2,1)}), bf16[32,64,3200]{2,1,0:T(8,128)(2,1)}, u32[]{:S(2)}, u32[]{:S(2)}) async-start(bf16[32,64,3200]{2,1,0:T(8,128)(2,1)} %stack.4), calls=%async_computation | async-start | bytes 26214400 | tf_op jit(solution)/shard_map/all_to_all | solution.py:18
  43.0 578.3 %copy-start.8 = (f32[256]{0:T(256)S(1)}, f32[256]{0:T(256)}, u32[]{:S(2)}) copy-start(f32[256]{0:T(256)} %param.35) | copy-start | bytes 3076
  43.9 579.3 %copy-start.1 = (bf16[384,2048]{1,0:T(8,128)(2,1)}, bf16[384,2048]{1,0:T(8,128)(2,1)S(1)}, u32[]{:S(2)}) copy-start(bf16[384,2048]{1,0:T(8,128)(2,1)S(1)} %fusion.37) | copy-start | bytes 4718596
  621.3 1.9 copy-start.11
  623.2 2.3 copy-start.12
  623.2 2.3 copy-start.2
  625.5 1.7 copy-start.13
  625.5 1.7 copy-start.14
  627.2 1.8 copy-start.3
  629.0 20.6 %copy-start.9 = (f32[256]{0:T(256)S(1)}, f32[256]{0:T(256)}, u32[]{:S(2)}) copy-start(f32[256]{0:T(256)} %param.37) | copy-start | bytes 3076
  629.0 20.6 %copy-start.10 = (f32[256]{0:T(256)S(1)}, f32[256]{0:T(256)}, u32[]{:S(2)}) copy-start(f32[256]{0:T(256)} %param.38) | copy-start | bytes 3076
  654.8 27.3 %all-to-all-start.2 = ((bf16[8,48,2048]{2,1,0:T(8,128)(2,1)}), bf16[8,48,2048]{2,1,0:T(8,128)(2,1)S(1)}, u32[]{:S(2)}, u32[]{:S(2)}) async-start(bf16[8,48,2048]{2,1,0:T(8,128)(2,1)} %bitcast.152), calls=%async_computation.2 | async-start | bytes 3145728 | tf_op jit(solution)/shard_map/all_to_all | solution.py:36
  661.5 21.0 %copy-start.5 = (f32[2048]{0:T(1024)S(1)}, f32[2048]{0:T(1024)}, u32[]{:S(2)}) copy-start(f32[2048]{0:T(1024)} %param.41) | copy-start | bytes 24580
  682.6 24.2 %copy-start.7 = (f32[1024]{0:T(1024)S(1)}, f32[1024]{0:T(1024)}, u32[]{:S(2)}) copy-start(f32[1024]{0:T(1024)} %param.43) | copy-start | bytes 12292
